TPU v7x, 32 devices: a whole 2x2x4 slice. The times are simulated.
32 devices in a mesh: sp: 8 (over z, y), tp: 4 (over x, core).
Axes of the slice: x: 2, y: 2, z: 4, core: 2. Of those that a mesh axis runs over, the one named last changes fastest.
Arguments:
- activations: bfloat16 [6144, 2048], P(('sp', 'tp')), may hold values from -6 to 6
- in_gain: float32 [2048], replicated, may hold values from 0.1 to 1.9
- w_pool_in: bfloat16 [2048, 1024], P(None, 'tp'), may hold values from -0.125 to 0.125
- pool_gain: float32 [1024], P('tp'), may hold values from 0.1 to 1.9
- w_qlat: bfloat16 [2048, 768], P(None, 'tp'), may hold values from -0.125 to 0.125
- w_kvlat: bfloat16 [2048, 512], P(None, 'tp'), may hold values from -0.125 to 0.125
- w_krope: bfloat16 [2048, 32], replicated, may hold values from -0.125 to 0.125
- qlat_gain: float32 [768], replicated, may hold values from 0.1 to 1.9
- kvlat_gain: float32 [512], replicated, may hold values from 0.1 to 1.9
- w_qup: bfloat16 [768, 1536], P(None, 'tp'), may hold values from -0.21875 to 0.21875
- w_kup: bfloat16 [512, 1024], P(None, 'tp'), may hold values from -0.25 to 0.25
- w_vup: bfloat16 [512, 1024], P(None, 'tp'), may hold values from -0.25 to 0.25
- qhead_gain: float32 [96], replicated, may hold values from 1.1 to 1.9
- khead_gain: float32 [96], replicated, may hold values from 1.1 to 1.9
- w_out_pool: bfloat16 [1024, 2048], P('tp'), may hold values from -0.1875 to 0.1875
- w_out_attn: bfloat16 [1024, 2048], P('tp'), may hold values from -0.75 to 0.75
Outputs:
- mixed: bfloat16 [6144, 2048], P(('sp', 'tp'))
All inputs are finite; a program needn't handle non-finite values.
Results may differ from a plain program's by a relative error of at most 0.025.
Values may be sent and summed in bfloat16 or wider, within the bound.
A program may use at most 128 MiB of HBM per device.

v0:
```python
import math
import jax
import jax.numpy as jnp
from jax import lax
from jax.sharding import PartitionSpec as P

GROUP = 256
NOPE = 64
ROPE = 32
VDIM = 64
QLAT = 768
KVLAT = 512
norm_eps = 1e-06
rope_theta = 10000.0
rim_depth = 15
block_rows = 512


def from_behind(block, axis, distance):
    devices = range(lax.axis_size(axis))
    route = [(i - distance, i) for i in devices if i - distance in devices]
    return lax.ppermute(block, axis, route)


def row_norm(source, norm_gain):
    as_float = source.astype(jnp.float32)
    factor = lax.rsqrt(jnp.mean(as_float * as_float, axis=-1, keepdims=True) + norm_eps)
    return as_float * factor * norm_gain


def rotate(head_rows, positions):
    half_rope = ROPE // 2
    frequency = rope_theta ** (-jnp.arange(0, ROPE, 2, dtype=jnp.float32) / ROPE)
    angles = positions.astype(jnp.float32)[:, None] * frequency[None, :]
    cosine = jnp.cos(angles)[:, None, :]
    sine_part = jnp.sin(angles)[:, None, :]
    plain_part = head_rows[..., :NOPE]
    lower_half = head_rows[..., NOPE : NOPE + half_rope]
    upper_half = head_rows[..., NOPE + half_rope :]
    return jnp.concatenate(
        [
            plain_part,
            lower_half * cosine - upper_half * sine_part,
            upper_half * cosine + lower_half * sine_part,
        ],
        axis=-1,
    )


def pool_mix(extended, positions, channel_start):
    row_count = positions.shape[0]
    width = extended.shape[1]
    channel = channel_start + jnp.arange(width, dtype=jnp.int32)
    window = jnp.left_shift(jnp.int32(2), channel // GROUP)
    as_float = extended.astype(jnp.float32)
    window_sum = jnp.zeros((row_count, width), jnp.float32)
    for lag_index in range(rim_depth + 1):
        lagged = as_float[rim_depth - lag_index : rim_depth - lag_index + row_count]
        window_sum = window_sum + jnp.where(lag_index < window[None, :], lagged, 0.0)
    divisor = jnp.minimum(positions[:, None] + 1, window[None, :]).astype(jnp.float32)
    return window_sum / divisor - as_float[rim_depth:]


def make_queries(q_normed, w_qup, norm_gain, positions):
    row_count = q_normed.shape[0]
    head_count = w_qup.shape[1] // (NOPE + ROPE)
    query_raw = jnp.dot(q_normed, w_qup, preferred_element_type=jnp.float32).astype(jnp.bfloat16)
    query_raw = query_raw.reshape(row_count, head_count, NOPE + ROPE)
    return rotate(row_norm(query_raw, norm_gain), positions).astype(jnp.bfloat16)


def plain_parts(kv_rows, w_kup, w_vup):
    key_plain = jnp.dot(kv_rows, w_kup, preferred_element_type=jnp.float32).astype(jnp.bfloat16)
    value_rows = jnp.dot(kv_rows, w_vup, preferred_element_type=jnp.float32).astype(jnp.bfloat16)
    return (key_plain, value_rows)


def finish_keys(key_plain, rope_rows, norm_gain, positions):
    row_count = key_plain.shape[0]
    head_count = key_plain.shape[1] // NOPE
    key_plain = key_plain.reshape(row_count, head_count, NOPE)
    shared = jnp.broadcast_to(rope_rows[:, None, :], (row_count, head_count, ROPE))
    joined = jnp.concatenate([key_plain, shared], axis=-1)
    key_rows = rotate(row_norm(joined, norm_gain), positions).astype(jnp.bfloat16)
    return key_rows.reshape(row_count, head_count * (NOPE + ROPE))


def update(state_pair, queries, query_pos, key_rows, value_rows, key_pos):
    numerator, denominator = state_pair
    head_count = queries.shape[1]
    key_rows = key_rows.reshape(key_rows.shape[0], head_count, NOPE + ROPE)
    value_rows = value_rows.reshape(value_rows.shape[0], head_count, VDIM)
    scores = jnp.einsum("qhd,khd->hqk", queries, key_rows, preferred_element_type=jnp.float32)
    scores = scores * (NOPE + ROPE) ** (-0.5)
    weights = jnp.where(key_pos[None, None, :] <= query_pos[None, :, None], jnp.exp(scores), 0.0)
    denominator = denominator + jnp.sum(weights, axis=-1)
    numerator = numerator + jnp.einsum(
        "hqk,khd->qhd", weights.astype(jnp.bfloat16), value_rows, preferred_element_type=jnp.float32
    )
    return (numerator, denominator)


def sweep(state_pair, pieces, expand, queries, query_pos):
    shard_rows = queries.shape[0]
    piece_rows = pieces[0].shape[0]
    block_size = shard_rows * math.gcd(piece_rows // shard_rows, max(1, block_rows // shard_rows))

    def advance(block_index, current):
        offset = block_index * block_size

        def accumulate(inner):
            chosen = tuple(
                (lax.dynamic_slice_in_dim(member, offset, block_size, 0) for member in pieces)
            )
            key_pos = offset + jnp.arange(block_size, dtype=jnp.int32)
            key_rows, value_rows = expand(chosen, key_pos)
            return update(inner, queries, query_pos, key_rows, value_rows, key_pos)

        def unchanged(inner):
            return inner

        return lax.cond(offset <= query_pos[-1], accumulate, unchanged, current)

    return lax.fori_loop(0, piece_rows // block_size, advance, state_pair)


def local(
    activations,
    in_gain,
    w_pool_in,
    pool_gain,
    w_qlat,
    w_kvlat,
    w_krope,
    qlat_gain,
    kvlat_gain,
    w_qup,
    w_kup,
    w_vup,
    qhead_gain,
    khead_gain,
    w_out_pool,
    w_out_attn,
):
    own_input = lax.all_gather(activations, "tp", axis=0, tiled=True)
    row_count = own_input.shape[0]
    positions = lax.axis_index("sp") * row_count + jnp.arange(row_count, dtype=jnp.int32)
    normed = row_norm(own_input, in_gain).astype(jnp.bfloat16)
    pool_in = jnp.dot(normed, w_pool_in, preferred_element_type=jnp.float32).astype(jnp.bfloat16)
    prev_rows = from_behind(pool_in[row_count - rim_depth :], "sp", 1)
    extended = jnp.concatenate([prev_rows, pool_in], axis=0)
    channel_start = lax.axis_index("tp") * pool_in.shape[1]
    pool_out = (pool_mix(extended, positions, channel_start) * pool_gain).astype(jnp.bfloat16)
    q_part = jnp.dot(normed, w_qlat, preferred_element_type=jnp.float32).astype(jnp.bfloat16)
    kv_part = jnp.dot(normed, w_kvlat, preferred_element_type=jnp.float32).astype(jnp.bfloat16)
    rope_key = jnp.dot(normed, w_krope, preferred_element_type=jnp.float32).astype(jnp.bfloat16)
    tp_index = lax.axis_index("tp")
    q_width = q_part.shape[1]
    kv_width = kv_part.shape[1]
    q_float = q_part.astype(jnp.float32)
    kv_float = kv_part.astype(jnp.float32)
    q_squares, kv_squares = lax.psum(
        (jnp.sum(q_float * q_float, axis=1), jnp.sum(kv_float * kv_float, axis=1)), "tp"
    )
    q_gain = lax.dynamic_slice_in_dim(qlat_gain, tp_index * q_width, q_width)
    kv_gain = lax.dynamic_slice_in_dim(kvlat_gain, tp_index * kv_width, kv_width)
    q_scaled = q_float * lax.rsqrt(q_squares / QLAT + norm_eps)[:, None] * q_gain
    kv_scaled = kv_float * lax.rsqrt(kv_squares / KVLAT + norm_eps)[:, None] * kv_gain
    q_normed, kv_normed = (
        lax.all_gather(q_scaled.astype(jnp.bfloat16), "tp", axis=1, tiled=True),
        lax.all_gather(kv_scaled.astype(jnp.bfloat16), "tp", axis=1, tiled=True),
    )
    queries = make_queries(q_normed, w_qup, qhead_gain, positions)
    head_count = queries.shape[1]
    start_pair = (
        jnp.zeros((row_count, head_count, VDIM), jnp.float32),
        jnp.zeros((head_count, row_count), jnp.float32),
    )
    key_plain, value_rows = plain_parts(kv_normed, w_kup, w_vup)

    def expand_plain(chosen, key_pos):
        return (finish_keys(chosen[0], chosen[2], khead_gain, key_pos), chosen[1])

    numerator, denominator = sweep(
        start_pair,
        (
            lax.all_gather(key_plain, "sp", axis=0, tiled=True),
            lax.all_gather(value_rows, "sp", axis=0, tiled=True),
            lax.all_gather(rope_key, "sp", axis=0, tiled=True),
        ),
        expand_plain,
        queries,
        positions,
    )
    attended = (numerator / jnp.transpose(denominator)[:, :, None]).astype(jnp.bfloat16)
    attended = attended.reshape(row_count, head_count * VDIM)
    term = jnp.dot(pool_out, w_out_pool, preferred_element_type=jnp.float32)
    return lax.psum_scatter(
        (term + jnp.dot(attended, w_out_attn, preferred_element_type=jnp.float32)).astype(
            jnp.bfloat16
        ),
        "tp",
        scatter_dimension=0,
        tiled=True,
    )


def solution(mesh):
    placed = (
        P(("sp", "tp"), None),
        P(),
        P(None, "tp"),
        P("tp"),
        P(None, "tp"),
        P(None, "tp"),
        P(),
        P(),
        P(),
        P(None, "tp"),
        P(None, "tp"),
        P(None, "tp"),
        P(),
        P(),
        P("tp", None),
        P("tp", None),
    )
    return jax.shard_map(
        local, mesh=mesh, in_specs=placed, out_specs=P(("sp", "tp"), None), check_vma=False
    )
```

profile of v0, /device:TPU:0, one launch (start us, length us, event | category | flops | bytes accessed | tf_op | source)
XLA Modules:
  0.0 318.9 jit_solution(7002376077708482121)
XLA Ops:
  8.1 32.1 %all-gather.5.cloned.1.call-done = bf16[768,2048]{1,0:T(8,128)(2,1)} async-done(((bf16[192,2048]{1,0:T(8,128)(2,1)}), bf16[768,2048]{1,0:T(8,128)(2,1)}) %all-gather.5.cloned.1.call-update) | async-done | bytes 3145744 | tf_op jit(solution)/shard_map/all_gather | solution.py:145
  40.2 2.7 fusion.23
  44.0 1.2 multiply_reduce_fusion.1
  45.7 1.2 multiply_reduce_fusion
  46.9 6.0 %all-reduce = (f32[768]{0:T(1024)S(1)}, f32[768]{0:T(1024)S(1)}) all-reduce(f32[768]{0:T(1024)S(1)} %get-tuple-element.242, f32[768]{0:T(1024)S(1)} %get-tuple-element.244), channel_id=1, replica_groups=mesh['sp'=8,'tp'=4] {'tp'}, use_global_device_ids=true, to_apply=%region_2.3 | all-reduce | flops 1536 | bytes 12288 | tf_op jit(solution)/shard_map/psum | solution.py:162
  54.8 8.7 %all_gather.19 = bf16[768,512]{0,1:T(8,128)(2,1)S(1)} all-gather(bf16[768,128]{0,1:T(8,128)(2,1)S(1)} %multiply_convert_fusion.1), channel_id=1, replica_groups=mesh['sp'=8,'tp'=4] {'tp'}, dimensions={1}, use_global_device_ids=true | all-gather | bytes 983040 | tf_op jit(solution)/shard_map/all_gather | solution.py:171
  63.5 1.2 convolution_convert_fusion.2
  64.8 2.1 convolution_convert_fusion.1
  67.5 3.1 convolution_convert_fusion.3
  70.6 3.4 %collective-permute-start = (bf16[15,256]{1,0:T(8,128)(2,1)S(1)}, bf16[15,256]{1,0:T(8,128)(2,1)S(1)}, u32[]{:S(2)}, u32[]{:S(2)}) collective-permute-start(bf16[15,256]{1,0:T(8,128)(2,1)S(1)} %slice.102), channel_id=1, source_target_pairs={{0,4},{4,8},{8,12},{12,16},{16,20},{20,24},{24,28},{1,5},{5,9},{9,... | collective-permute-start | bytes 23048 | tf_op jit(solution)/shard_map/ppermute | solution.py:22
  75.1 32.1 %all_gather.22 = bf16[6144,32]{0,1:T(8,128)(2,1)S(1)} all-gather(bf16[768,32]{0,1:T(8,128)(2,1)S(1)} %convolution_convert_fusion.6), channel_id=1, replica_groups=mesh['sp'=8,'tp'=4] {'sp'}, dimensions={0}, use_global_device_ids=true | all-gather | bytes 442368 | tf_op jit(solution)/shard_map/all_gather | solution.py:189
  107.3 5.2 %fusion.49 = f32[768,2048]{1,0:T(8,128)} fusion(bf16[256,2048]{1,0:T(8,128)(2,1)S(1)} %copy-done, f32[783,256]{1,0:T(8,128)S(1)} %maximum_convert_fusion, f32[256]{0:T(256)S(1)} %copy-done.15, s32[256]{0:T(256)S(1)} %fusion.69, s32[768]{0:T(1024)S(1)} %fusion.68, pred[256]{0:T(512)(128)(4,1)S(1)} %get-tuple-element.246, ...), kind=kOutput, calls=%fused_computation.95 | convolution fusion | flops 812580864 | bytes 19937280 | tf_op jit(solution)/shard_map/dot_general | solution.py:197
  112.6 2.0 convolution_convert_fusion
  115.8 20.9 %all-gather.7.cloned.1.call-done = bf16[6144,256]{1,0:T(8,128)(2,1)} async-done(((bf16[768,256]{1,0:T(8,128)(2,1)}), bf16[6144,256]{1,0:T(8,128)(2,1)}) %all-gather.7.cloned.1.call-update) | async-done | bytes 3145744 | tf_op jit(solution)/shard_map/all_gather | solution.py:188
  136.7 4.6 %copy.18 = bf16[6144,256]{0,1:T(8,128)(2,1)} copy(bf16[6144,256]{1,0:T(8,128)(2,1)} %all-gather.7.cloned.1.call-done) | data formatting | bytes 6291456 | tf_op jit(solution)/shard_map/while | solution.py:124
  141.3 56.1 %all-gather.9.cloned.1.call-done = bf16[6144,256]{1,0:T(8,128)(2,1)} async-done(((bf16[768,256]{1,0:T(8,128)(2,1)}), bf16[6144,256]{1,0:T(8,128)(2,1)}) %all-gather.9.cloned.1.call-update) | async-done | bytes 3145744 | tf_op jit(solution)/shard_map/all_gather | solution.py:187
  197.5 4.7 %copy.19 = bf16[6144,256]{0,1:T(8,128)(2,1)} copy(bf16[6144,256]{1,0:T(8,128)(2,1)} %all-gather.9.cloned.1.call-done) | data formatting | bytes 6291456 | tf_op jit(solution)/shard_map/while | solution.py:124
  202.2 17.4 %while.15 = (s32[]{:T(128)}, f32[768,4,64]{0,2,1:T(8,128)S(1)}, f32[4,768]{1,0:T(4,128)S(1)}, s32[768]{0:T(1024)S(1)}, bf16[6144,256]{0,1:T(8,128)(2,1)}, /*inde...) while((s32[]{:T(128)}, f32[768,4,64]{0,2,1:T(8,128)S(1)}, ...), condition=%wide.region_11.12_spmd, body=%wide.region_6.11_spmd.sunk | while | flops 775635520 | bytes 32112456 | solution.py:124
  203.5 7.2 %conditional.2 = ((f32[768,4,64]{0,2,1:T(8,128)S(1)}, f32[4,768]{1,0:T(4,128)S(1)})) conditional(s32[]{:T(128)} %convert_element_type.159, (f32[768,4,64]{0,2,1:T(8,128)S(1)}, f32[4,768]{1,0:T(4,128)S(1)}) %tuple.55, (s32[]{:T(128)}, bf16[6144,256]{0,1:T(8,128)(2,1)}, s32[768]{0:T(1024)S(1)}, bf16[6144,256]{0,1:T(8,128)(2,1)}, ...), branch_computations={%region_7.7_spmd, %region_8.10_spmd} | conditional | flops 775635520 | bytes 32112226 | solution.py:122
  203.6 1.2 constant_dynamic-slice_fusion.1
  205.9 2.6 fusion
  208.6 2.1 fusion.8
  219.7 5.5 %add_convert_fusion.1 = bf16[768,2048]{1,0:T(8,128)(2,1)} fusion(f32[768,2048]{1,0:T(8,128)} %fusion.49, bf16[768,256]{0,1:T(8,128)(2,1)S(1)} %bitcast.48, bf16[256,2048]{1,0:T(8,128)(2,1)S(1)} %copy-done.4), kind=kOutput, calls=%fused_computation.39 | convolution fusion | flops 808452096 | bytes 10878976 | tf_op jit(solution)/shard_map/dot_general | solution.py:199
  225.2 87.2 %reduce-scatter.2.cloned.1.call-done = bf16[192,2048]{1,0:T(8,128)(2,1)} async-done(((bf16[768,2048]{1,0:T(8,128)(2,1)}), bf16[192,2048]{1,0:T(8,128)(2,1)}) %reduce-scatter.2.cloned.1.call-update) | async-done | bytes 786448 | tf_op jit(solution)/shard_map/reduce_scatter | solution.py:198
  (105 shorter events, 14.2 us)
Async XLA Ops:
  6.5 100.8 %copy-start = (bf16[256,2048]{1,0:T(8,128)(2,1)S(1)}, bf16[256,2048]{1,0:T(8,128)(2,1)}, u32[]{:S(2)}) copy-start(bf16[256,2048]{1,0:T(8,128)(2,1)} %param.34) | copy-start | bytes 3145732
  6.5 36.4 %copy-start.9 = (f32[2048]{0:T(1024)S(1)}, f32[2048]{0:T(1024)}, u32[]{:S(2)}) copy-start(f32[2048]{0:T(1024)} %param.21) | copy-start | bytes 24580
  6.5 33.6 %all-gather.5.cloned.1.call-start = ((), (), s32[]{:S(2)}) async-start(), calls=%async_computation.1 | async-start | bytes 3932160 | tf_op jit(solution)/shard_map/all_gather | solution.py:145
  7.3 105.3 %all-gather.11.cloned.1.call-start = ((), (), s32[]{:S(2)}) async-start(), calls=%async_computation.4 | async-start | bytes 1474560 | tf_op jit(solution)/shard_map/all_gather | solution.py:170
  40.2 2.8 copy-start.3
  43.0 1.0 copy-start.6
  44.0 2.9 copy-start.1
  44.0 1.7 copy-start.12
  45.7 17.8 %copy-start.14 = (bf16[512,256]{1,0:T(8,128)(2,1)S(1)}, bf16[512,256]{1,0:T(8,128)(2,1)}, u32[]{:S(2)}) copy-start(bf16[512,256]{1,0:T(8,128)(2,1)} %param.31) | copy-start | bytes 786436
  53.8 13.7 %copy-start.11 = (bf16[2048,256]{1,0:T(8,128)(2,1)S(1)}, bf16[2048,256]{1,0:T(8,128)(2,1)}, u32[]{:S(2)}) copy-start(bf16[2048,256]{1,0:T(8,128)(2,1)} %param.22) | copy-start | bytes 3145732
  53.8 82.9 %all-gather.7.cloned.1.call-start = ((), (), s32[]{:S(2)}) async-start(), calls=%async_computation.2 | async-start | bytes 3538944 | tf_op jit(solution)/shard_map/all_gather | solution.py:188
  64.7 132.7 %all-gather.9.cloned.1.call-start = ((), (), s32[]{:S(2)}) async-start(), calls=%async_computation.3 | async-start | bytes 3538944 | tf_op jit(solution)/shard_map/all_gather | solution.py:187
  66.9 245.4 %reduce-scatter.2.cloned.1.call-start = ((), (), s32[]{:S(2)}) async-start(), calls=%async_computation.5 | async-start | bytes 3932160 | tf_op jit(solution)/shard_map/reduce_scatter | solution.py:198
  67.5 6.6 %copy-start.2 = (bf16[768,2048]{1,0:T(8,128)(2,1)S(1)}, bf16[768,2048]{1,0:T(8,128)(2,1)}, u32[]{:S(2)}) copy-start(bf16[768,2048]{1,0:T(8,128)(2,1)} %copy-done.1) | copy-start | bytes 9437188
  67.5 6.6 %copy-start.7 = (bf16[2048,32]{0,1:T(8,128)(2,1)S(1)}, bf16[2048,32]{0,1:T(8,128)(2,1)}, u32[]{:S(2)}) copy-start(bf16[2048,32]{0,1:T(8,128)(2,1)} %param.26) | copy-start | bytes 393220
  70.6 36.7 %copy-start.15 = (f32[256]{0:T(256)S(1)}, f32[256]{0:T(256)}, u32[]{:S(2)}) copy-start(f32[256]{0:T(256)} %param.23) | copy-start | bytes 3076
  70.6 36.6 %collective-permute-start = (bf16[15,256]{1,0:T(8,128)(2,1)S(1)}, bf16[15,256]{1,0:T(8,128)(2,1)S(1)}, u32[]{:S(2)}, u32[]{:S(2)}) collective-permute-start(bf16[15,256]{1,0:T(8,128)(2,1)S(1)} %slice.102), channel_id=1, source_target_pairs={{0,4},{4,8},{8,12},{12,16},{16,20},{20,24},{24,28},{1,5},{5,9},{9,... | collective-permute-start | bytes 23048 | tf_op jit(solution)/shard_map/ppermute | solution.py:22
  107.3 5.2 %copy-start.13 = (bf16[768,384]{1,0:T(8,128)(2,1)S(1)}, bf16[768,384]{1,0:T(8,128)(2,1)}, u32[]{:S(2)}) copy-start(bf16[768,384]{1,0:T(8,128)(2,1)} %param.29) | copy-start | bytes 1769476
  112.6 2.1 copy-start.10
  141.3 60.9 %copy-start.8 = (f32[96]{0:T(128)S(1)}, f32[96]{0:T(128)}, u32[]{:S(2)}) copy-start(f32[96]{0:T(128)} %param.33) | copy-start | bytes 1156
  202.2 17.4 %copy-start.4 = (bf16[256,2048]{1,0:T(8,128)(2,1)S(1)}, bf16[256,2048]{1,0:T(8,128)(2,1)}, u32[]{:S(2)}) copy-start(bf16[256,2048]{1,0:T(8,128)(2,1)} %param.35) | copy-start | bytes 3145732
  203.5 2.4 copy-start.5
Sparse Core Ops, SparseCore 0:
  8.9 31.2 all-gather.4
  53.9 18.5 all-gather.10
  74.7 61.9 all-gather.6
  138.7 58.6 all-gather.8
  225.3 86.9 reduce-scatter.1
where the time goes:
time: 320 us; the launch traced here: 319 us
  waiting for transfers between devices  197 us (62%)
  blocking collectives  46.9 us (15%)
  matrix products  27.2 us (8%)
  local copies, waits for them, and re-layouts  18.1 us (6%)
  between operations  13.5 us (4%)
  other arithmetic  7.26 us (2%)
  loops' own time  5.33 us (2%)
  starting transfers between devices  3.61 us (1%)
    reduce_scatter x1, waiting for transfers between devices, local(): lax.psum_scatter((term + jnp.dot(attended, w_out_attn, preferred_element_...  87.2 us
    all_gather x1, waiting for transfers between devices, local(): lax.all_gather(key_plain, 'sp', axis=0, tiled=True)  56.1 us
    all_gather x1, blocking collectives, local(): lax.all_gather(rope_key, 'sp', axis=0, tiled=True)  32.1 us
    all_gather x1, waiting for transfers between devices, local(): own_input = lax.all_gather(activations, 'tp', axis=0, tiled=True)  32.1 us
    all_gather x1, waiting for transfers between devices, local(): lax.all_gather(value_rows, 'sp', axis=0, tiled=True)  20.9 us
    while x2, local copies, waits for them, and re-layouts, sweep(): return lax.fori_loop(0, piece_rows // block_size, advance, state_pair)  9.32 us
    all_gather x1, blocking collectives, local(): lax.all_gather(kv_scaled.astype(jnp.bfloat16), 'tp', axis=1, tiled=True)  8.73 us
  transfers between devices with their start and end apart: 6, of which 4 were waited for; matrix products, arithmetic and copies ran while one was open for 7% of the time, Pallas kernels for 0%

commit v1 on v0

--- a/solution.py
+++ b/solution.py
@@ -142,7 +142,12 @@
     w_out_pool,
     w_out_attn,
 ):
-    own_input = lax.all_gather(activations, "tp", axis=0, tiled=True)
+    ring = [activations]
+    for hop in range(3):
+        ring.append(lax.ppermute(ring[-1], "tp", [(dev, (dev + 1) % 4) for dev in range(4)]))
+    own_input = jnp.roll(
+        jnp.concatenate(ring[::-1], axis=0), (lax.axis_index("tp") + 1) * ring[0].shape[0], axis=0
+    )
     row_count = own_input.shape[0]
     positions = lax.axis_index("sp") * row_count + jnp.arange(row_count, dtype=jnp.int32)
     normed = row_norm(own_input, in_gain).astype(jnp.bfloat16)

time: 320 us -> 324 us (1.012)
  local copies, waits for them, and re-layouts: 18.1 us -> 21.4 us
    ppermute x0 -> x3, waiting for transfers between devices: none -> 34 us  [local(): lax.ppermute(ring[-1], 'tp', [(dev, (dev + 1) % 4) for dev in range(4)])]
    all_gather x1 -> x0, waiting for transfers between devices: 32.1 us -> none  [local(): own_input = lax.all_gather(activations, 'tp', axis=0, tiled=True)]
  transfers between devices with their start and end apart: 6 -> 8, of which waited for: 4 -> 6; matrix products, arithmetic and copies ran while one was open for 7% -> 7% of each run, Pallas kernels for 0% -> 0%
where the time goes in v1:
time: 324 us
  waiting for transfers between devices  198 us (61%)
  blocking collectives  48.2 us (15%)
  matrix products  28.2 us (9%)
  local copies, waits for them, and re-layouts  21.4 us (7%)
  between operations  13.6 us (4%)
  loops' own time  5.42 us (2%)
  other arithmetic  5.02 us (2%)
  starting transfers between devices  4.2 us (1%)
    reduce_scatter x1, waiting for transfers between devices, local(): lax.psum_scatter((term + jnp.dot(attended, w_out_attn, preferred_element_...  87.1 us
    all_gather x1, waiting for transfers between devices, local(): lax.all_gather(key_plain, 'sp', axis=0, tiled=True)  56.2 us
    ppermute x3, waiting for transfers between devices, local(): lax.ppermute(ring[-1], 'tp', [(dev, (dev + 1) % 4) for dev in range(4)])  34 us
    all_gather x1, blocking collectives, local(): lax.all_gather(rope_key, 'sp', axis=0, tiled=True)  32.9 us
    all_gather x1, waiting for transfers between devices, local(): lax.all_gather(value_rows, 'sp', axis=0, tiled=True)  20.3 us
    all_gather x1, blocking collectives, local(): lax.all_gather(kv_scaled.astype(jnp.bfloat16), 'tp', axis=1, tiled=True)  9.41 us
    while x2, local copies, waits for them, and re-layouts, sweep(): return lax.fori_loop(0, piece_rows // block_size, advance, state_pair)  9.4 us
  transfers between devices with their start and end apart: 8, of which 6 were waited for; matrix products, arithmetic and copies ran while one was open for 7% of the time, Pallas kernels for 0%

profile of v1, /device:TPU:0, one launch (start us, length us, event | category | flops | bytes accessed | tf_op | source)
XLA Modules:
  0.0 323.7 jit_solution(10146911001589171603)
XLA Ops:
  7.0 11.8 %collective-permute-done = bf16[192,2048]{1,0:T(8,128)(2,1)S(1)} collective-permute-done((bf16[192,2048]{1,0:T(8,128)(2,1)}, bf16[192,2048]{1,0:T(8,128)(2,1)S(1)}, u32[]{:S(2)}, u32[]{:S(2)}) %collective-permute-start) | collective-permute-done | bytes 786464 | tf_op jit(solution)/shard_map/ppermute | solution.py:147
  18.9 11.4 %collective-permute-done.1 = bf16[192,2048]{1,0:T(8,128)(2,1)S(1)} collective-permute-done((bf16[192,2048]{1,0:T(8,128)(2,1)S(1)}, bf16[192,2048]{1,0:T(8,128)(2,1)S(1)}, u32[]{:S(2)}, u32[]{:S(2)}) %collective-permute-start.1) | collective-permute-done | bytes 786464 | tf_op jit(solution)/shard_map/ppermute | solution.py:147
  31.0 10.8 %collective-permute-done.2 = bf16[192,2048]{1,0:T(8,128)(2,1)} collective-permute-done((bf16[192,2048]{1,0:T(8,128)(2,1)S(1)}, bf16[192,2048]{1,0:T(8,128)(2,1)}, u32[]{:S(2)}, u32[]{:S(2)}) %collective-permute-start.2) | collective-permute-done | bytes 786464 | tf_op jit(solution)/shard_map/ppermute | solution.py:147
  45.8 1.3 fusion.23
  47.1 1.7 multiply_reduce_fusion.1
  48.9 1.7 multiply_reduce_fusion
  50.5 5.9 %all-reduce = (f32[768]{0:T(1024)S(1)}, f32[768]{0:T(1024)S(1)}) all-reduce(f32[768]{0:T(1024)S(1)} %get-tuple-element.242, f32[768]{0:T(1024)S(1)} %get-tuple-element.244), channel_id=1, replica_groups=mesh['sp'=8,'tp'=4] {'tp'}, use_global_device_ids=true, to_apply=%region_2.3 | all-reduce | flops 1536 | bytes 12288 | tf_op jit(solution)/shard_map/psum | solution.py:167
  58.2 9.4 %all_gather.15 = bf16[768,512]{0,1:T(8,128)(2,1)S(1)} all-gather(bf16[768,128]{0,1:T(8,128)(2,1)S(1)} %multiply_convert_fusion.1), channel_id=1, replica_groups=mesh['sp'=8,'tp'=4] {'tp'}, dimensions={1}, use_global_device_ids=true | all-gather | bytes 983040 | tf_op jit(solution)/shard_map/all_gather | solution.py:176
  70.6 3.7 %convolution_convert_fusion.3 = bf16[768,256]{1,0:T(8,128)(2,1)S(1)} fusion(bf16[2048,256]{1,0:T(8,128)(2,1)} %param.22, f32[2048]{0:T(1024)S(1)} %copy-done.13, f32[768]{0:T(1024)S(1)} %add_rsqrt_fusion.4, bf16[1536,2048]{1,0:T(8,128)(2,1)} %copy-done.2, s32[]{:T(128)S(6)} %select_n.136), kind=kOutput, calls=%fused_computation.45 | convolution fusion | flops 811794432 | bytes 4598788 | tf_op jit(solution)/shard_map/dot_general | solution.py:154
  74.4 3.6 %collective-permute-start.3 = (bf16[15,256]{1,0:T(8,128)(2,1)S(1)}, bf16[15,256]{1,0:T(8,128)(2,1)S(1)}, u32[]{:S(2)}, u32[]{:S(2)}) collective-permute-start(bf16[15,256]{1,0:T(8,128)(2,1)S(1)} %slice.102), channel_id=1, source_target_pairs={{0,4},{4,8},{8,12},{12,16},{16,20},{20,24},{24,28},{1,5},{5,9},{9,... | collective-permute-start | bytes 23048 | tf_op jit(solution)/shard_map/ppermute | solution.py:22
  78.0 1.4 convolution_convert_fusion.6
  79.4 32.9 %all_gather.18 = bf16[6144,32]{0,1:T(8,128)(2,1)S(1)} all-gather(bf16[768,32]{0,1:T(8,128)(2,1)S(1)} %convolution_convert_fusion.6), channel_id=1, replica_groups=mesh['sp'=8,'tp'=4] {'sp'}, dimensions={0}, use_global_device_ids=true | all-gather | bytes 442368 | tf_op jit(solution)/shard_map/all_gather | solution.py:194
  112.4 5.2 %fusion.49 = f32[768,2048]{1,0:T(8,128)} fusion(bf16[256,2048]{1,0:T(8,128)(2,1)S(1)} %copy-done, f32[783,256]{1,0:T(8,128)S(1)} %maximum_convert_fusion, f32[256]{0:T(256)S(1)} %copy-done.14, s32[256]{0:T(256)S(1)} %fusion.69, s32[768]{0:T(1024)S(1)} %fusion.68, pred[256]{0:T(512)(128)(4,1)S(1)} %get-tuple-element.246, ...), kind=kOutput, calls=%fused_computation.95 | convolution fusion | flops 812580864 | bytes 19937280 | tf_op jit(solution)/shard_map/dot_general | solution.py:202
  117.6 2.0 convolution_convert_fusion
  120.9 20.3 %all-gather.4.cloned.1.call-done = bf16[6144,256]{1,0:T(8,128)(2,1)} async-done(((bf16[768,256]{1,0:T(8,128)(2,1)}), bf16[6144,256]{1,0:T(8,128)(2,1)}) %all-gather.4.cloned.1.call-update) | async-done | bytes 3145744 | tf_op jit(solution)/shard_map/all_gather | solution.py:193
  141.2 4.7 %copy.18 = bf16[6144,256]{0,1:T(8,128)(2,1)} copy(bf16[6144,256]{1,0:T(8,128)(2,1)} %all-gather.4.cloned.1.call-done) | data formatting | bytes 6291456 | tf_op jit(solution)/shard_map/while | solution.py:124
  146.0 56.2 %all-gather.6.cloned.1.call-done = bf16[6144,256]{1,0:T(8,128)(2,1)} async-done(((bf16[768,256]{1,0:T(8,128)(2,1)}), bf16[6144,256]{1,0:T(8,128)(2,1)}) %all-gather.6.cloned.1.call-update) | async-done | bytes 3145744 | tf_op jit(solution)/shard_map/all_gather | solution.py:192
  202.1 4.6 %copy.19 = bf16[6144,256]{0,1:T(8,128)(2,1)} copy(bf16[6144,256]{1,0:T(8,128)(2,1)} %all-gather.6.cloned.1.call-done) | data formatting | bytes 6291456 | tf_op jit(solution)/shard_map/while | solution.py:124
  206.9 17.6 %while.15 = (s32[]{:T(128)}, f32[768,4,64]{0,2,1:T(8,128)S(1)}, f32[4,768]{1,0:T(4,128)S(1)}, s32[768]{0:T(1024)S(1)}, bf16[6144,256]{0,1:T(8,128)(2,1)}, /*inde...) while((s32[]{:T(128)}, f32[768,4,64]{0,2,1:T(8,128)S(1)}, ...), condition=%wide.region_11.12_spmd, body=%wide.region_6.11_spmd.sunk | while | flops 775635520 | bytes 32112456 | solution.py:124
  208.2 7.2 %conditional.2 = ((f32[768,4,64]{0,2,1:T(8,128)S(1)}, f32[4,768]{1,0:T(4,128)S(1)})) conditional(s32[]{:T(128)} %convert_element_type.175, (f32[768,4,64]{0,2,1:T(8,128)S(1)}, f32[4,768]{1,0:T(4,128)S(1)}) %tuple.55, (s32[]{:T(128)}, bf16[6144,256]{0,1:T(8,128)(2,1)}, s32[768]{0:T(1024)S(1)}, bf16[6144,256]{0,1:T(8,128)(2,1)}, ...), branch_computations={%region_7.7_spmd, %region_8.10_spmd} | conditional | flops 775635520 | bytes 32112226 | solution.py:122
  210.6 2.6 fusion
  213.3 2.1 fusion.8
  224.6 5.5 %add_convert_fusion.1 = bf16[768,2048]{1,0:T(8,128)(2,1)} fusion(f32[768,2048]{1,0:T(8,128)} %fusion.49, bf16[768,256]{0,1:T(8,128)(2,1)S(1)} %bitcast.46, bf16[256,2048]{1,0:T(8,128)(2,1)S(1)} %copy-done.3), kind=kOutput, calls=%fused_computation.39 | convolution fusion | flops 808452096 | bytes 10878976 | tf_op jit(solution)/shard_map/dot_general | solution.py:204
  230.1 87.1 %reduce-scatter.2.cloned.1.call-done = bf16[192,2048]{1,0:T(8,128)(2,1)} async-done(((bf16[768,2048]{1,0:T(8,128)(2,1)}), bf16[192,2048]{1,0:T(8,128)(2,1)}) %reduce-scatter.2.cloned.1.call-update) | async-done | bytes 786448 | tf_op jit(solution)/shard_map/reduce_scatter | solution.py:203
  (118 shorter events, 18.9 us)
Async XLA Ops:
  6.5 105.8 %copy-start = (bf16[256,2048]{1,0:T(8,128)(2,1)S(1)}, bf16[256,2048]{1,0:T(8,128)(2,1)}, u32[]{:S(2)}) copy-start(bf16[256,2048]{1,0:T(8,128)(2,1)} %param.34) | copy-start | bytes 3145732
  6.5 39.2 %copy-start.1 = (bf16[192,2048]{1,0:T(8,128)(2,1)S(1)}, bf16[192,2048]{1,0:T(8,128)(2,1)}, u32[]{:S(2)}) copy-start(bf16[192,2048]{1,0:T(8,128)(2,1)} %param.20) | copy-start | bytes 2359300
  6.5 111.1 %all-gather.8.cloned.1.call-start = ((), (), s32[]{:S(2)}) async-start(), calls=%async_computation.3 | async-start | bytes 1474560 | tf_op jit(solution)/shard_map/all_gather | solution.py:175
  6.5 12.3 %collective-permute-start = (bf16[192,2048]{1,0:T(8,128)(2,1)}, bf16[192,2048]{1,0:T(8,128)(2,1)S(1)}, u32[]{:S(2)}, u32[]{:S(2)}) collective-permute-start(bf16[192,2048]{1,0:T(8,128)(2,1)} %param.20), channel_id=1, source_target_pairs={{0,1},{1,2},{2,3},{3,0},{4,5},{5,6},{6,7},{7,4},{8,9},{9,10},{10,1... | collective-permute-start | bytes 2359304 | tf_op jit(solution)/shard_map/ppermute | solution.py:147
  18.9 11.4 %collective-permute-start.1 = (bf16[192,2048]{1,0:T(8,128)(2,1)S(1)}, bf16[192,2048]{1,0:T(8,128)(2,1)S(1)}, u32[]{:S(2)}, u32[]{:S(2)}) collective-permute-start(bf16[192,2048]{1,0:T(8,128)(2,1)S(1)} %collective-permute-done), channel_id=1, source_target_pairs={{0,1},{1,2},{2,3},{3,0},{4,5},{5,6},{6,7},{7,4},{8,9},{9,10},{10,1... | collective-permute-start | bytes 2359304 | tf_op jit(solution)/shard_map/ppermute | solution.py:147
  30.3 11.5 %collective-permute-start.2 = (bf16[192,2048]{1,0:T(8,128)(2,1)S(1)}, bf16[192,2048]{1,0:T(8,128)(2,1)}, u32[]{:S(2)}, u32[]{:S(2)}) collective-permute-start(bf16[192,2048]{1,0:T(8,128)(2,1)S(1)} %collective-permute-done.1), channel_id=1, source_target_pairs={{0,1},{1,2},{2,3},{3,0},{4,5},{5,6},{6,7},{7,4},{8,9},{9,10},{10,1... | collective-permute-start | bytes 2359304 | tf_op jit(solution)/shard_map/ppermute | solution.py:147
  43.1 4.1 %copy-start.9 = (bf16[2048,128]{1,0:T(8,128)(2,1)S(1)}, bf16[2048,128]{1,0:T(8,128)(2,1)}, u32[]{:S(2)}) copy-start(bf16[2048,128]{1,0:T(8,128)(2,1)} %param.25) | copy-start | bytes 1572868
  43.1 4.1 %copy-start.13 = (f32[2048]{0:T(1024)S(1)}, f32[2048]{0:T(1024)}, u32[]{:S(2)}) copy-start(f32[2048]{0:T(1024)} %param.21) | copy-start | bytes 24580
  45.7 3.2 copy-start.7
  45.8 4.7 %copy-start.2 = (bf16[1536,2048]{1,0:T(8,128)(2,1)}, bf16[1536,2048]{1,0:T(8,128)(2,1)S(1)}, u32[]{:S(2)}) copy-start(bf16[1536,2048]{1,0:T(8,128)(2,1)S(1)} %constant_dynamic-update-slice_fusion) | copy-start | bytes 18874372
  48.8 18.8 %copy-start.10 = (bf16[512,256]{1,0:T(8,128)(2,1)S(1)}, bf16[512,256]{1,0:T(8,128)(2,1)}, u32[]{:S(2)}) copy-start(bf16[512,256]{1,0:T(8,128)(2,1)} %param.31) | copy-start | bytes 786436
  48.8 20.1 %copy-start.11 = (bf16[512,256]{1,0:T(8,128)(2,1)S(1)}, bf16[512,256]{1,0:T(8,128)(2,1)}, u32[]{:S(2)}) copy-start(bf16[512,256]{1,0:T(8,128)(2,1)} %param.30) | copy-start | bytes 786436
  57.3 83.9 %all-gather.4.cloned.1.call-start = ((), (), s32[]{:S(2)}) async-start(), calls=%async_computation.1 | async-start | bytes 3538944 | tf_op jit(solution)/shard_map/all_gather | solution.py:193
  68.8 133.3 %all-gather.6.cloned.1.call-start = ((), (), s32[]{:S(2)}) async-start(), calls=%async_computation.2 | async-start | bytes 3538944 | tf_op jit(solution)/shard_map/all_gather | solution.py:192
  70.1 7.9 %slice-start = ((s8[6291456]{0:T(1024)(128)(4,1)}), s8[2097152]{0:T(1024)(128)(4,1)S(1)}, s32[]{:S(2)}) async-start(s8[6291456]{0:T(1024)(128)(4,1)} %bitcast.42), calls=%async_computation.5 | async-start | bytes 4194304
  70.1 7.9 %copy-start.12 = (bf16[2048,32]{0,1:T(8,128)(2,1)S(1)}, bf16[2048,32]{0,1:T(8,128)(2,1)}, u32[]{:S(2)}) copy-start(bf16[2048,32]{0,1:T(8,128)(2,1)} %param.26) | copy-start | bytes 393220
  70.1 247.1 %reduce-scatter.2.cloned.1.call-start = ((), (), s32[]{:S(2)}) async-start(), calls=%async_computation.4 | async-start | bytes 3932160 | tf_op jit(solution)/shard_map/reduce_scatter | solution.py:203
  70.6 7.3 %slice-start.1 = ((s8[6291456]{0:T(1024)(128)(4,1)}), s8[4194304]{0:T(1024)(128)(4,1)S(1)}, s32[]{:S(2)}) async-start(s8[6291456]{0:T(1024)(128)(4,1)} %bitcast.42), calls=%async_computation.6 | async-start | bytes 8388608
  74.3 38.0 %copy-start.14 = (f32[256]{0:T(256)S(1)}, f32[256]{0:T(256)}, u32[]{:S(2)}) copy-start(f32[256]{0:T(256)} %param.23) | copy-start | bytes 3076
  74.4 37.9 %collective-permute-start.3 = (bf16[15,256]{1,0:T(8,128)(2,1)S(1)}, bf16[15,256]{1,0:T(8,128)(2,1)S(1)}, u32[]{:S(2)}, u32[]{:S(2)}) collective-permute-start(bf16[15,256]{1,0:T(8,128)(2,1)S(1)} %slice.102), channel_id=1, source_target_pairs={{0,4},{4,8},{8,12},{12,16},{16,20},{20,24},{24,28},{1,5},{5,9},{9,... | collective-permute-start | bytes 23048 | tf_op jit(solution)/shard_map/ppermute | solution.py:22
  112.4 5.3 %copy-start.8 = (bf16[768,384]{1,0:T(8,128)(2,1)S(1)}, bf16[768,384]{1,0:T(8,128)(2,1)}, u32[]{:S(2)}) copy-start(bf16[768,384]{1,0:T(8,128)(2,1)} %param.29) | copy-start | bytes 1769476
  112.4 7.4 %copy-start.6 = (f32[96]{0:T(128)S(1)}, f32[96]{0:T(128)}, u32[]{:S(2)}) copy-start(f32[96]{0:T(128)} %param.32) | copy-start | bytes 1156
  120.9 85.9 %copy-start.5 = (f32[96]{0:T(128)S(1)}, f32[96]{0:T(128)}, u32[]{:S(2)}) copy-start(f32[96]{0:T(128)} %param.33) | copy-start | bytes 1156
  206.9 17.7 %copy-start.3 = (bf16[256,2048]{1,0:T(8,128)(2,1)S(1)}, bf16[256,2048]{1,0:T(8,128)(2,1)}, u32[]{:S(2)}) copy-start(bf16[256,2048]{1,0:T(8,128)(2,1)} %param.35) | copy-start | bytes 3145732
  (1 other events, 2.4 us)
Sparse Core Ops, SparseCore 0:
  57.4 19.5 all-gather.7
  79.2 61.9 all-gather.3
  143.4 58.6 all-gather.5
  230.2 86.9 reduce-scatter.1
